TPU v7x, 256 devices: a whole 4x4x8 slice. The times are simulated.
256 devices in a mesh: ep: 32 (over z, x), tp: 8 (over y, core).
Axes of the slice: x: 4, y: 4, z: 8, core: 2. Of those that a mesh axis runs over, the one named last changes fastest.
Arguments:
- tokens: bfloat16 [768, 4096], P('ep'), may hold values from -6 to 6
- delta_state: float32 [768, 16, 128, 128], P('ep', 'tp'), may hold values from -0.625 to 0.625
- attn_gain: float32 [4096], replicated, may hold values from 0.1 to 1.9
- query_weight: bfloat16 [4096, 2048], P('ep', 'tp'), may hold values from -0.09375 to 0.09375
- key_weight: bfloat16 [4096, 2048], P('ep', 'tp'), may hold values from -0.09375 to 0.09375
- value_weight: bfloat16 [4096, 2048], P('ep', 'tp'), may hold values from -0.09375 to 0.09375
- decay_weight: bfloat16 [4096, 16], replicated, may hold values from -0.09375 to 0.09375
- beta_weight: bfloat16 [4096, 16], replicated, may hold values from -0.09375 to 0.09375
- decay_rate: float32 [16], P('tp'), may hold values from 0.05 to 3
- head_gain: float32 [128], replicated, may hold values from 0.1 to 1.9
- output_weight: bfloat16 [2048, 4096], P('tp'), may hold values from -0.125 to 0.125
- ffn_gain: float32 [4096], replicated, may hold values from 0.1 to 1.9
- expert_ids: int32 [768, 2], P('ep'), may hold values from 0 to 31, all different within a row; in each aligned block of 24 rows (0 to 23, 24 to 47, ...) at most 3 rows name the same one
- group_prob: float32 [768], P('ep'), may hold values from 0.3 to 1
- expert_logit: float32 [768, 2], P('ep'), may hold values from -8 to 8
- expert_gate: bfloat16 [32, 4096, 1024], P('ep', None, 'tp'), may hold values from -0.09375 to 0.09375
- expert_up: bfloat16 [32, 4096, 1024], P('ep', None, 'tp'), may hold values from -0.09375 to 0.09375
- expert_down: bfloat16 [32, 1024, 4096], P('ep', 'tp'), may hold values from -0.1875 to 0.1875
- dense_gate: bfloat16 [4096, 4096], P('tp', 'ep'), may hold values from -0.09375 to 0.09375
- dense_up: bfloat16 [4096, 4096], P('tp', 'ep'), may hold values from -0.09375 to 0.09375
- dense_down: bfloat16 [4096, 4096], P('ep', 'tp'), may hold values from -0.09375 to 0.09375
- dense_mix: float32 [4096], P('tp'), may hold values from -3 to 3
Outputs:
- mixed_out: bfloat16 [768, 4096], P('ep', 'tp')
- new_state: float32 [768, 16, 128, 128], P('ep', 'tp')
Inputs may be any that keep to these rules, and one draw needn't show every extreme that they name: `expert_ids`: each row names 2 different experts. Among the rows of one device (aligned blocks of 24 rows) no expert is named by more than 3 rows, and in every draw some expert reaches 3 in some block.
All inputs are finite; a program needn't handle non-finite values.
Results may differ from a plain program's by a relative error of at most 0.02.
Values may be sent and summed in bfloat16 or wider, within the bound.
No kernel may reach another device: no remote copies, remote signals or barrier semaphores. Data moves between devices by JAX's collectives and lax.ppermute only.
A program may use at most 64 MiB of HBM per device.

v0:
```python
import jax
import jax.numpy as jnp
from jax import lax
from jax.sharding import PartitionSpec as P

EPS = 1e-06


def split_up(shard, dim, count):
    shape = shard.shape
    tiles = shard.reshape(*shape[:dim], count, shape[dim] // count, *shape[dim + 1 :])
    return jnp.moveaxis(tiles, dim, 0)


def summed_on_arrival(shard, axis, dim):
    tiles = split_up(shard, dim, lax.axis_size(axis))
    arrived = lax.all_to_all(tiles, axis, split_axis=0, concat_axis=0, tiled=True)
    return arrived.astype(jnp.float32).sum(axis=0)


def sent_to_all(shard, axis):
    count = lax.axis_size(axis)
    return lax.all_to_all(
        jnp.broadcast_to(shard[None], (count, *shard.shape)), axis, 0, 0, tiled=True
    )


def over_copies(shard, axis):
    everything = sent_to_all(shard, axis)
    return jnp.sum(everything.astype(jnp.float32), axis=0)


def laid_out(tiles, dim):
    shape = list(tiles.shape[1:])
    shape[dim] *= tiles.shape[0]
    return jnp.moveaxis(tiles, 0, dim).reshape(shape)


def collect(shard, axis, dim):
    return laid_out(sent_to_all(shard, axis), dim)


def rms_scale(values, gain):
    mean_sq = jnp.mean(values * values, axis=-1, keepdims=True)
    return values * lax.rsqrt(mean_sq + EPS) * gain


def unit_rows(values):
    return values * lax.rsqrt(jnp.sum(values * values, axis=-1, keepdims=True) + EPS)


def per_device(
    tokens,
    delta_state,
    attn_gain,
    query_weight,
    key_weight,
    value_weight,
    decay_weight,
    beta_weight,
    decay_rate,
    head_gain,
    output_weight,
    ffn_gain,
    expert_ids,
    group_prob,
    expert_logit,
    expert_gate,
    expert_up,
    expert_down,
    dense_gate,
    dense_up,
    dense_down,
    dense_mix,
):
    seq_rows = tokens.shape[0]
    head_count = delta_state.shape[1]
    head_size = delta_state.shape[2]
    width_local = head_count * head_size
    tp_index = lax.axis_index("tp")
    residual = tokens.astype(jnp.float32)
    normed = rms_scale(residual, attn_gain).astype(jnp.bfloat16)
    spread = lax.all_to_all(normed, "ep", split_axis=1, concat_axis=0, tiled=True)
    joined = jnp.concatenate((query_weight, key_weight, value_weight), axis=1)
    summed = summed_on_arrival(
        jnp.dot(spread, joined, preferred_element_type=jnp.float32).astype(jnp.bfloat16), "ep", 0
    )
    query_sum = summed[:, :width_local]
    key_sum = summed[:, width_local : 2 * width_local]
    value_sum = summed[:, 2 * width_local :]

    def heads_of(values):
        rounded = lax.optimization_barrier(values.astype(jnp.bfloat16))
        return rounded.astype(jnp.float32).reshape(seq_rows, head_count, head_size)

    query_unit = unit_rows(heads_of(query_sum)) * head_size ** (-0.5)
    key_unit = unit_rows(heads_of(key_sum))
    value_heads = heads_of(value_sum)
    decay_cols = lax.dynamic_slice_in_dim(decay_weight, tp_index * head_count, head_count, 1)
    beta_cols = lax.dynamic_slice_in_dim(beta_weight, tp_index * head_count, head_count, 1)
    decay_pre = jnp.dot(normed, decay_cols, preferred_element_type=jnp.float32)
    decay = jnp.exp(-decay_rate * jax.nn.softplus(decay_pre))
    beta_gate = jax.nn.sigmoid(jnp.dot(normed, beta_cols, preferred_element_type=jnp.float32))
    recalled = jnp.einsum("bhk,bhkv->bhv", key_unit, delta_state)
    correction = beta_gate[..., None] * (value_heads - decay[..., None] * recalled)
    new_state = (
        decay[..., None, None] * delta_state + key_unit[..., :, None] * correction[..., None, :]
    )
    read_out = jnp.einsum("bhk,bhkv->bhv", query_unit, new_state)
    head_out = rms_scale(read_out, head_gain).astype(jnp.bfloat16).reshape(seq_rows, width_local)
    attn_part = jnp.dot(head_out, output_weight, preferred_element_type=jnp.float32)
    attn_sum = over_copies(attn_part.astype(jnp.bfloat16), "tp").astype(jnp.float32)
    middle = residual + attn_sum
    ffn_in = rms_scale(middle, ffn_gain).astype(jnp.bfloat16)
    slice_width = dense_gate.shape[0]
    hidden_width = dense_gate.shape[1]
    own_columns = lax.dynamic_slice_in_dim(ffn_in, tp_index * slice_width, slice_width, 1)
    gate_up = jnp.concatenate((dense_gate, dense_up), axis=1)
    dense_part = jnp.dot(collect(own_columns, "ep", 0), gate_up, preferred_element_type=jnp.float32)
    dense_sum = over_copies(dense_part.astype(jnp.bfloat16), "tp").astype(jnp.float32)
    dense_hidden = (jax.nn.silu(dense_sum[:, :hidden_width]) * dense_sum[:, hidden_width:]).astype(
        jnp.bfloat16
    )
    dense_out = summed_on_arrival(
        jnp.dot(dense_hidden, dense_down, preferred_element_type=jnp.float32).astype(jnp.bfloat16),
        "ep",
        0,
    )
    expert_count = lax.axis_size("ep")
    top_count = expert_ids.shape[1]
    capacity = max(2, 2 * seq_rows * top_count // expert_count)
    pair_ids = expert_ids.reshape(-1)
    onehot = (pair_ids[:, None] == jnp.arange(expert_count, dtype=jnp.int32)[None, :]).astype(
        jnp.int32
    )
    ranks = jnp.sum(onehot * (jnp.cumsum(onehot, axis=0) - 1), axis=1)
    places = pair_ids * capacity + ranks
    dispatch = (
        jnp.arange(expert_count * capacity, dtype=jnp.int32)[:, None] == places[None, :]
    ).astype(jnp.bfloat16)
    repeated = jnp.repeat(ffn_in, top_count, axis=0)
    outgoing = jnp.dot(dispatch, repeated, preferred_element_type=jnp.float32).astype(jnp.bfloat16)
    outgoing = outgoing.reshape(expert_count, capacity, ffn_in.shape[1])
    arrived = lax.all_to_all(outgoing, "ep", split_axis=0, concat_axis=0, tiled=True)
    gate_vals = jnp.einsum(
        "snd,df->snf", arrived, expert_gate[0], preferred_element_type=jnp.float32
    )
    up_vals = jnp.einsum("snd,df->snf", arrived, expert_up[0], preferred_element_type=jnp.float32)
    expert_hidden = (jax.nn.silu(gate_vals) * up_vals).astype(jnp.bfloat16)
    partial_value = jnp.einsum(
        "snf,fd->snd", expert_hidden, expert_down[0], preferred_element_type=jnp.float32
    )
    summed_cols = summed_on_arrival(partial_value.astype(jnp.bfloat16), "tp", 2)
    returned = lax.all_to_all(
        summed_cols.astype(jnp.bfloat16), "ep", split_axis=0, concat_axis=0, tiled=True
    )
    flat_back = returned.reshape(expert_count * capacity, slice_width)
    picked = (
        jnp.take(flat_back, places, axis=0)
        .astype(jnp.float32)
        .reshape(seq_rows, top_count, slice_width)
    )
    logit_exp = jnp.exp(expert_logit)
    route_weight = group_prob[:, None] * logit_exp / jnp.sum(logit_exp, axis=1, keepdims=True)
    expert_mix = jnp.sum(route_weight[..., None] * picked, axis=1)
    own_middle = lax.dynamic_slice_in_dim(middle, tp_index * slice_width, slice_width, 1)
    mixed_out = (own_middle + jax.nn.sigmoid(dense_mix) * dense_out + expert_mix).astype(
        jnp.bfloat16
    )
    return (mixed_out, new_state)


def solution(mesh):
    return jax.shard_map(
        per_device,
        mesh=mesh,
        in_specs=(
            P("ep", None),
            P("ep", "tp", None, None),
            P(),
            P("ep", "tp"),
            P("ep", "tp"),
            P("ep", "tp"),
            P(),
            P(),
            P("tp"),
            P(),
            P("tp", None),
            P(),
            P("ep", None),
            P("ep"),
            P("ep", None),
            P("ep", None, "tp"),
            P("ep", None, "tp"),
            P("ep", "tp", None),
            P("tp", "ep"),
            P("tp", "ep"),
            P("ep", "tp"),
            P("tp"),
        ),
        out_specs=(P("ep", "tp"), P("ep", "tp", None, None)),
        check_vma=False,
    )
```

profile of v0, /device:TPU:2, one launch (start us, length us, event | category | flops | bytes accessed | tf_op | source)
XLA Modules:
  0.0 269.3 jit_solution(17994246620742949373)
XLA Ops:
  0.7 1.2 fusion.12
  1.9 1.1 copy_bitcast_fusion
  3.0 21.2 %all_to_all.59 = bf16[24,32,128]{2,0,1:T(8,128)(2,1)S(1)} all-to-all(bf16[24,32,128]{2,0,1:T(8,128)(2,1)S(1)} %copy_bitcast_fusion), channel_id=1, replica_groups=mesh['ep'=32,'tp'=8] {'ep'}, dimensions={1} | all-to-all | bytes 393216 | tf_op jit(solution)/shard_map/all_to_all | solution.py:83
  24.2 2.4 convolution_convert_fusion.3
  26.6 5.7 %all-to-all-start.1 = ((bf16[32,24,768]{2,1,0:T(8,128)(2,1)}), bf16[32,24,768]{2,1,0:T(8,128)(2,1)S(1)}, u32[]{:S(2)}, u32[]{:S(2)}) async-start(bf16[32,24,768]{2,1,0:T(8,128)(2,1)} %bitcast.60), calls=%async_computation.1 | async-start | bytes 2359296 | tf_op jit(solution)/shard_map/all_to_all | solution.py:17
  32.3 1.1 fusion.40
  33.5 1.1 fusion.3
  34.6 0.1 copy.116
  34.7 27.5 %all-to-all-done.1 = bf16[32,24,768]{2,1,0:T(8,128)(2,1)S(1)} async-done(((bf16[32,24,768]{2,1,0:T(8,128)(2,1)}), bf16[32,24,768]{2,1,0:T(8,128)(2,1)S(1)}, u32[]{:S(2)}, u32[]{:S(2)}) %all-to-all-start.1) | async-done | bytes 1179680 | tf_op jit(solution)/shard_map/all_to_all | solution.py:17
  62.2 0.2 reduce.1
  62.4 0.1 multiply_reduce_fusion.4
  62.6 0.1 multiply_multiply_fusion
  62.7 0.1 multiply_reduce_fusion.3
  62.8 0.1 broadcast_multiply_fusion
  62.9 2.6 fusion.54
  65.5 0.1 subtract_multiply_fusion
  65.6 1.1 multiply_add_fusion
  66.8 1.6 copy-done.2
  68.4 0.5 fusion.55
  68.9 0.1 multiply_reduce_fusion.2
  69.1 0.1 multiply_convert_fusion.1
  69.2 0.4 convolution_convert_fusion.2
  69.6 1.3 broadcast_in_dim.15
  70.9 4.6 %all-to-all-start.2 = ((bf16[8,24,4096]{2,1,0:T(8,128)(2,1)}), bf16[8,24,4096]{2,1,0:T(8,128)(2,1)}, u32[]{:S(2)}, u32[]{:S(2)}) async-start(bf16[8,24,4096]{2,1,0:T(8,128)(2,1)} %broadcast_in_dim.15), calls=%async_computation.2 | async-start | bytes 3145728 | tf_op jit(solution)/shard_map/all_to_all | solution.py:23
  75.6 0.1 reshape.169
  75.8 0.2 select_reduce_fusion
  76.0 21.1 %all-to-all-done.2 = bf16[8,24,4096]{2,1,0:T(8,128)(2,1)} async-done(((bf16[8,24,4096]{2,1,0:T(8,128)(2,1)}), bf16[8,24,4096]{2,1,0:T(8,128)(2,1)}, u32[]{:S(2)}, u32[]{:S(2)}) %all-to-all-start.2) | async-done | bytes 1572896 | tf_op jit(solution)/shard_map/all_to_all | solution.py:23
  97.2 1.7 convert_reduce_fusion.1
  98.8 0.2 multiply_reduce_fusion
  99.0 0.1 multiply_convert_fusion
  99.1 0.3 broadcast_in_dim.19
  99.5 0.3 copy-done.5
  99.8 0.9 reshape.170
  100.7 1.3 convolution_convert_fusion.1
  102.0 1.3 reshape.171
  103.3 5.6 %all-to-all-start.6 = ((bf16[32,3,4096]{2,1,0:T(4,128)(2,1)}), bf16[32,3,4096]{2,1,0:T(4,128)(2,1)S(1)}, u32[]{:S(2)}, u32[]{:S(2)}) async-start(bf16[32,3,4096]{2,1,0:T(4,128)(2,1)} %reshape.171), calls=%async_computation.6 | async-start | bytes 2097152 | tf_op jit(solution)/shard_map/all_to_all | solution.py:144
  108.9 1.4 constant_dynamic-slice_fusion
  110.3 26.4 %all-to-all-done.6 = bf16[32,3,4096]{2,1,0:T(4,128)(2,1)S(1)} async-done(((bf16[32,3,4096]{2,1,0:T(4,128)(2,1)}), bf16[32,3,4096]{2,1,0:T(4,128)(2,1)S(1)}, u32[]{:S(2)}, u32[]{:S(2)}) %all-to-all-start.6) | async-done | bytes 786464 | tf_op jit(solution)/shard_map/all_to_all | solution.py:144
  136.7 1.7 broadcast_in_dim.16
  138.4 5.6 %all-to-all-start.3 = ((bf16[32,24,512]{2,1,0:T(8,128)(2,1)}), bf16[32,24,512]{2,1,0:T(8,128)(2,1)}, u32[]{:S(2)}, u32[]{:S(2)}) async-start(bf16[32,24,512]{2,1,0:T(8,128)(2,1)} %broadcast_in_dim.16), calls=%async_computation.3 | async-start | bytes 1572864 | tf_op jit(solution)/shard_map/all_to_all | solution.py:23
  144.0 2.6 fusion.7
  146.6 3.6 %convolution_convert_fusion = bf16[32,3,4096]{2,0,1:T(8,128)(2,1)} fusion(bf16[1,128,4096]{2,1,0:T(8,128)(2,1)} %param.39, bf16[1,4096,128]{2,1,0:T(8,128)(2,1)} %param.38, bf16[32,3,4096]{2,1,0:T(4,128)(2,1)S(1)} %all-to-all-done.6, f32[32,3,128]{2,0,1:T(8,128)} %fusion.7), kind=kOutput, calls=%fused_computation.2 | convolution fusion | flops 201793536 | bytes 3719168 | tf_op jit(solution)/shard_map/snf,fd->snd/dot_general | solution.py:150
  150.2 2.2 copy.150
  152.3 12.9 %all-to-all-done.3 = bf16[32,24,512]{2,1,0:T(8,128)(2,1)} async-done(((bf16[32,24,512]{2,1,0:T(8,128)(2,1)}), bf16[32,24,512]{2,1,0:T(8,128)(2,1)}, u32[]{:S(2)}, u32[]{:S(2)}) %all-to-all-start.3) | async-done | bytes 786464 | tf_op jit(solution)/shard_map/all_to_all | solution.py:23
  165.2 3.5 %all-to-all-start.7 = ((bf16[8,32,3,512]{3,1,2,0:T(8,128)(2,1)}), bf16[8,32,3,512]{3,1,2,0:T(8,128)(2,1)S(1)}, u32[]{:S(2)}, u32[]{:S(2)}) async-start(bf16[8,32,3,512]{3,1,2,0:T(8,128)(2,1)} %bitcast.62), calls=%async_computation.7 | async-start | bytes 1572864 | tf_op jit(solution)/shard_map/all_to_all | solution.py:17
  168.8 2.2 convolution_convert_fusion.5
  171.1 10.8 %all-to-all-done.7 = bf16[8,32,3,512]{3,1,2,0:T(8,128)(2,1)S(1)} async-done(((bf16[8,32,3,512]{3,1,2,0:T(8,128)(2,1)}), bf16[8,32,3,512]{3,1,2,0:T(8,128)(2,1)S(1)}, u32[]{:S(2)}, u32[]{:S(2)}) %all-to-all-start.7) | async-done | bytes 786464 | tf_op jit(solution)/shard_map/all_to_all | solution.py:17
  181.8 2.9 %broadcast_in_dim.17 = bf16[8,768,256]{2,1,0:T(8,128)(2,1)} broadcast(bf16[768,256]{1,0:T(8,128)(2,1)} %convolution_convert_fusion.5), dimensions={1,2} | broadcast | bytes 3538944 | tf_op jit(solution)/shard_map/broadcast_in_dim | solution.py:24
  184.7 4.4 %all-to-all-start.4 = ((bf16[8,768,256]{2,1,0:T(8,128)(2,1)}), bf16[8,768,256]{2,1,0:T(8,128)(2,1)}, u32[]{:S(2)}, u32[]{:S(2)}) async-start(bf16[8,768,256]{2,1,0:T(8,128)(2,1)} %broadcast_in_dim.17), calls=%async_computation.4 | async-start | bytes 6291456 | tf_op jit(solution)/shard_map/all_to_all | solution.py:23
  189.2 0.1 reduce_sum.136
  189.3 0.7 copy.128
  190.0 37.5 %all-to-all-done.4 = bf16[8,768,256]{2,1,0:T(8,128)(2,1)} async-done(((bf16[8,768,256]{2,1,0:T(8,128)(2,1)}), bf16[8,768,256]{2,1,0:T(8,128)(2,1)}, u32[]{:S(2)}, u32[]{:S(2)}) %all-to-all-start.4) | async-done | bytes 3145760 | tf_op jit(solution)/shard_map/all_to_all | solution.py:23
  227.6 5.6 %all-to-all-start.8 = ((bf16[32,3,512]{2,1,0:T(4,128)(2,1)}), bf16[32,3,512]{2,1,0:T(4,128)(2,1)S(1)}, u32[]{:S(2)}, u32[]{:S(2)}) async-start(bf16[32,3,512]{2,1,0:T(4,128)(2,1)} %copy.128), calls=%async_computation.8 | async-start | bytes 262144 | tf_op jit(solution)/shard_map/all_to_all | solution.py:154
  233.2 2.4 convert_reduce_fusion
  235.6 1.3 convolution_convert_fusion.4
  236.8 5.2 %all-to-all-done.8 = bf16[32,3,512]{2,1,0:T(4,128)(2,1)S(1)} async-done(((bf16[32,3,512]{2,1,0:T(4,128)(2,1)}), bf16[32,3,512]{2,1,0:T(4,128)(2,1)S(1)}, u32[]{:S(2)}, u32[]{:S(2)}) %all-to-all-start.8) | async-done | bytes 98336 | tf_op jit(solution)/shard_map/all_to_all | solution.py:154
  242.0 5.5 %all-to-all-start.5 = ((bf16[32,24,512]{2,1,0:T(8,128)(2,1)}), bf16[32,24,512]{2,1,0:T(8,128)(2,1)S(1)}, u32[]{:S(2)}, u32[]{:S(2)}) async-start(bf16[32,24,512]{2,1,0:T(8,128)(2,1)} %bitcast.64), calls=%async_computation.5 | async-start | bytes 1572864 | tf_op jit(solution)/shard_map/all_to_all | solution.py:17
  247.7 0.1 mul.260
  247.9 0.1 copy.123
  248.2 0.7 gather_fusion
  248.9 0.2 multiply_reduce_fusion.1
  249.2 19.4 %all-to-all-done.5 = bf16[32,24,512]{2,1,0:T(8,128)(2,1)S(1)} async-done(((bf16[32,24,512]{2,1,0:T(8,128)(2,1)}), bf16[32,24,512]{2,1,0:T(8,128)(2,1)S(1)}, u32[]{:S(2)}, u32[]{:S(2)}) %all-to-all-start.5) | async-done | bytes 786464 | tf_op jit(solution)/shard_map/all_to_all | solution.py:17
  268.6 0.1 convert_reduce_fusion.2
  268.7 0.6 add_convert_fusion
  (60 shorter events, 1.0 us)
Async XLA Ops:
  0.6 68.5 %copy-start = (bf16[256,4096]{1,0:T(8,128)(2,1)S(1)}, bf16[256,4096]{1,0:T(8,128)(2,1)}, u32[]{:S(2)}) copy-start(bf16[256,4096]{1,0:T(8,128)(2,1)} %param.32) | copy-start | bytes 6291460
  0.6 31.6 %copy-start.3 = (bf16[24,4096]{1,0:T(8,128)(2,1)S(1)}, bf16[24,4096]{1,0:T(8,128)(2,1)}, u32[]{:S(2)}) copy-start(bf16[24,4096]{1,0:T(8,128)(2,1)} %param.22) | copy-start | bytes 589828
  0.7 31.6 %copy-start.6 = (f32[4096]{0:T(1024)S(1)}, f32[4096]{0:T(1024)}, u32[]{:S(2)}) copy-start(f32[4096]{0:T(1024)} %param.24) | copy-start | bytes 49156
  0.7 31.6 %copy-start.16 = (f32[2]{0:T(128)S(1)}, f32[2]{0:T(128)}, u32[]{:S(2)}) copy-start(f32[2]{0:T(128)} %param.30) | copy-start | bytes 28
  26.6 35.7 %all-to-all-start.1 = ((bf16[32,24,768]{2,1,0:T(8,128)(2,1)}), bf16[32,24,768]{2,1,0:T(8,128)(2,1)S(1)}, u32[]{:S(2)}, u32[]{:S(2)}) async-start(bf16[32,24,768]{2,1,0:T(8,128)(2,1)} %bitcast.60), calls=%async_computation.1 | async-start | bytes 2359296 | tf_op jit(solution)/shard_map/all_to_all | solution.py:17
  62.7 2.9 %copy-start.1 = (f32[24,2,128,128]{3,2,1,0:T(8,128)S(1)}, f32[24,2,128,128]{3,2,1,0:T(8,128)}, u32[]{:S(2)}) copy-start(f32[24,2,128,128]{3,2,1,0:T(8,128)} %param.23) | copy-start | bytes 9437188
  66.7 1.7 copy-start.2
  66.7 2.3 copy-start.11
  69.2 6.3 %copy-start.8 = (s32[24,2]{0,1:T(2,128)S(1)}, s32[24,2]{0,1:T(2,128)}, u32[]{:S(2)}) copy-start(s32[24,2]{0,1:T(2,128)} %param.34) | copy-start | bytes 580
  69.6 29.3 %copy-start.4 = (bf16[24,4096]{1,0:T(8,128)(2,1)S(1)}, bf16[24,4096]{1,0:T(8,128)(2,1)}, u32[]{:S(2)}) copy-start(bf16[24,4096]{1,0:T(8,128)(2,1)} %param.22) | copy-start | bytes 589828
  70.9 28.1 %copy-start.7 = (f32[4096]{0:T(1024)S(1)}, f32[4096]{0:T(1024)}, u32[]{:S(2)}) copy-start(f32[4096]{0:T(1024)} %param.33) | copy-start | bytes 49156
  70.9 26.3 %all-to-all-start.2 = ((bf16[8,24,4096]{2,1,0:T(8,128)(2,1)}), bf16[8,24,4096]{2,1,0:T(8,128)(2,1)}, u32[]{:S(2)}, u32[]{:S(2)}) async-start(bf16[8,24,4096]{2,1,0:T(8,128)(2,1)} %broadcast_in_dim.15), calls=%async_computation.2 | async-start | bytes 3145728 | tf_op jit(solution)/shard_map/all_to_all | solution.py:23
  99.1 0.7 copy-start.5
  103.3 33.3 %all-to-all-start.6 = ((bf16[32,3,4096]{2,1,0:T(4,128)(2,1)}), bf16[32,3,4096]{2,1,0:T(4,128)(2,1)S(1)}, u32[]{:S(2)}, u32[]{:S(2)}) async-start(bf16[32,3,4096]{2,1,0:T(4,128)(2,1)} %reshape.171), calls=%async_computation.6 | async-start | bytes 2097152 | tf_op jit(solution)/shard_map/all_to_all | solution.py:144
  138.4 26.9 %all-to-all-start.3 = ((bf16[32,24,512]{2,1,0:T(8,128)(2,1)}), bf16[32,24,512]{2,1,0:T(8,128)(2,1)}, u32[]{:S(2)}, u32[]{:S(2)}) async-start(bf16[32,24,512]{2,1,0:T(8,128)(2,1)} %broadcast_in_dim.16), calls=%async_computation.3 | async-start | bytes 1572864 | tf_op jit(solution)/shard_map/all_to_all | solution.py:23
  150.2 18.6 %copy-start.13 = (bf16[512,128]{1,0:T(8,128)(2,1)S(1)}, bf16[512,128]{1,0:T(8,128)(2,1)}, u32[]{:S(2)}) copy-start(bf16[512,128]{1,0:T(8,128)(2,1)} %param.41) | copy-start | bytes 393220
  150.2 18.6 %copy-start.14 = (bf16[512,128]{1,0:T(8,128)(2,1)S(1)}, bf16[512,128]{1,0:T(8,128)(2,1)}, u32[]{:S(2)}) copy-start(bf16[512,128]{1,0:T(8,128)(2,1)} %param.40) | copy-start | bytes 393220
  165.2 16.6 %all-to-all-start.7 = ((bf16[8,32,3,512]{3,1,2,0:T(8,128)(2,1)}), bf16[8,32,3,512]{3,1,2,0:T(8,128)(2,1)S(1)}, u32[]{:S(2)}, u32[]{:S(2)}) async-start(bf16[8,32,3,512]{3,1,2,0:T(8,128)(2,1)} %bitcast.62), calls=%async_computation.7 | async-start | bytes 1572864 | tf_op jit(solution)/shard_map/all_to_all | solution.py:17
  184.7 42.9 %all-to-all-start.4 = ((bf16[8,768,256]{2,1,0:T(8,128)(2,1)}), bf16[8,768,256]{2,1,0:T(8,128)(2,1)}, u32[]{:S(2)}, u32[]{:S(2)}) async-start(bf16[8,768,256]{2,1,0:T(8,128)(2,1)} %broadcast_in_dim.17), calls=%async_computation.4 | async-start | bytes 6291456 | tf_op jit(solution)/shard_map/all_to_all | solution.py:23
  189.3 46.3 %copy-start.15 = (bf16[128,512]{1,0:T(8,128)(2,1)S(1)}, bf16[128,512]{1,0:T(8,128)(2,1)}, u32[]{:S(2)}) copy-start(bf16[128,512]{1,0:T(8,128)(2,1)} %param.42) | copy-start | bytes 393220
  227.6 14.4 %all-to-all-start.8 = ((bf16[32,3,512]{2,1,0:T(4,128)(2,1)}), bf16[32,3,512]{2,1,0:T(4,128)(2,1)S(1)}, u32[]{:S(2)}, u32[]{:S(2)}) async-start(bf16[32,3,512]{2,1,0:T(4,128)(2,1)} %copy.128), calls=%async_computation.8 | async-start | bytes 262144 | tf_op jit(solution)/shard_map/all_to_all | solution.py:154
  233.1 14.8 %copy-start.10 = (f32[24,2]{0,1:T(2,128)S(1)}, f32[24,2]{0,1:T(2,128)}, u32[]{:S(2)}) copy-start(f32[24,2]{0,1:T(2,128)} %param.36) | copy-start | bytes 580
  233.1 14.9 %copy-start.12 = (f32[24]{0:T(128)S(1)}, f32[24]{0:T(128)}, u32[]{:S(2)}) copy-start(f32[24]{0:T(128)} %param.35) | copy-start | bytes 292
  233.2 15.0 %copy-start.9 = (f32[512]{0:T(512)S(1)}, f32[512]{0:T(512)}, u32[]{:S(2)}) copy-start(f32[512]{0:T(512)} %param.43) | copy-start | bytes 6148
  242.0 26.6 %all-to-all-start.5 = ((bf16[32,24,512]{2,1,0:T(8,128)(2,1)}), bf16[32,24,512]{2,1,0:T(8,128)(2,1)S(1)}, u32[]{:S(2)}, u32[]{:S(2)}) async-start(bf16[32,24,512]{2,1,0:T(8,128)(2,1)} %bitcast.64), calls=%async_computation.5 | async-start | bytes 1572864 | tf_op jit(solution)/shard_map/all_to_all | solution.py:17
where the time goes:
time: 271 us; the launch traced here: 269 us
  waiting for transfers between devices  161 us (59%)
  starting transfers between devices  40.5 us (15%)
  blocking collectives  21.2 us (8%)
  matrix products  19.1 us (7%)
  local copies, waits for them, and re-layouts  16.5 us (6%)
  other arithmetic  10.1 us (4%)
    all_to_all x3, waiting for transfers between devices, sent_to_all(): lax.all_to_all(jnp.broadcast_to(shard[None], (count, *shard.shape)), axis...  71.6 us
    all_to_all x3, waiting for transfers between devices, summed_on_arrival(): lax.all_to_all(tiles, axis, split_axis=0, concat_axis=0, tiled=True)  57.7 us
    all_to_all x1, waiting for transfers between devices, per_device(): lax.all_to_all(outgoing, 'ep', split_axis=0, concat_axis=0, tiled=True)  26.4 us
    all_to_all x1, blocking collectives, per_device(): lax.all_to_all(normed, 'ep', split_axis=1, concat_axis=0, tiled=True)  21.2 us
    all_to_all x3, starting transfers between devices, summed_on_arrival(): lax.all_to_all(tiles, axis, split_axis=0, concat_axis=0, tiled=True)  14.7 us
    all_to_all x3, starting transfers between devices, sent_to_all(): lax.all_to_all(jnp.broadcast_to(shard[None], (count, *shard.shape)), axis...  14.7 us
    broadcast_in_dim x3, local copies, waits for them, and re-layouts, sent_to_all(): jnp.broadcast_to(shard[None], (count, *shard.shape))  5.88 us
    all_to_all x1, starting transfers between devices, per_device(): lax.all_to_all(summed_cols.astype(jnp.bfloat16), 'ep', split_axis=0, conc...  5.56 us
  transfers between devices with their start and end apart: 8, of which 8 were waited for; matrix products, arithmetic and copies ran while one was open for 8% of the time, Pallas kernels for 0%

commit v1 on v0

v1 whole, which is shorter than its diff:
```python
import jax
import jax.numpy as jnp
from jax import lax
from jax.sharding import Mesh, PartitionSpec as P

EPS = 1e-06
BF = jnp.bfloat16
F32 = jnp.float32
NZ, NX, NT = 8, 4, 8
CAP = 3


def exchange(tiles, axes):
    return lax.all_to_all(tiles, axes, split_axis=0, concat_axis=0, tiled=True)


def gathered(shard, axis):
    count = lax.axis_size(axis)
    return exchange(jnp.broadcast_to(shard[None], (count, *shard.shape)), axis)


def two_parts(values):
    high = lax.reduce_precision(values, 8, 7)
    return high.astype(BF), (values - high).astype(BF)


def unit_rows(values):
    return values * lax.rsqrt(jnp.sum(values * values, axis=-1, keepdims=True) + EPS)


def rms_scale(values, gain):
    mean_sq = jnp.mean(values * values, axis=-1, keepdims=True)
    return values * lax.rsqrt(mean_sq + EPS) * gain


def per_device(
    tokens,
    delta_state,
    attn_gain,
    query_weight,
    key_weight,
    value_weight,
    decay_weight,
    beta_weight,
    decay_rate,
    head_gain,
    output_weight,
    ffn_gain,
    expert_ids,
    group_prob,
    expert_logit,
    expert_gate,
    expert_up,
    expert_down,
    dense_gate,
    dense_up,
    dense_down,
    dense_mix,
):
    rows, width = tokens.shape
    heads, size = delta_state.shape[1:3]
    cols = heads * size
    block = width // NT
    zi = lax.axis_index("z")
    ti = lax.axis_index("y") * 2 + lax.axis_index("c")

    qkv_weight = gathered(jnp.concatenate((query_weight, key_weight, value_weight), axis=1), "x")
    qkv_weight = qkv_weight.reshape(block, 3 * cols)
    half = dense_gate.shape[1]
    dense_all = gathered(
        jnp.concatenate(
            (
                jnp.concatenate((dense_gate, dense_up), axis=1),
                dense_down[:, : block // 2],
                dense_down[:, block // 2 :],
            ),
            axis=0,
        ),
        "x",
    )
    gate_up = dense_all[:, :block]
    down = jnp.concatenate((dense_all[:, block : block + half], dense_all[:, block + half :]), axis=2)

    pair_ids = expert_ids.reshape(-1)
    experts = jnp.arange(NZ * NX, dtype=jnp.int32)
    onehot = (pair_ids[:, None] == experts[None, :]).astype(F32)
    count = rows * 2
    earlier = jnp.arange(count)[:, None] > jnp.arange(count)[None, :]
    before = jnp.dot(earlier.astype(F32), onehot, preferred_element_type=F32)
    ranks = jnp.sum(onehot * before, axis=1)
    places = (pair_ids.astype(F32) * CAP + ranks).reshape(rows, 2)
    logit_exp = jnp.exp(expert_logit)
    route = group_prob[:, None] * logit_exp / jnp.sum(logit_exp, axis=1, keepdims=True)
    route_high, route_low = two_parts(route)
    meta = jnp.concatenate((places.astype(BF).T, route_high.T, route_low.T, jnp.zeros((2, rows), BF)), 0)
    meta = jnp.where(jnp.arange(NZ)[None, :, None] == zi, meta[:, None, :], 0).reshape(8, NZ * rows)
    meta = jnp.pad(meta, ((0, 0), (0, block - NZ * rows)))

    residual = tokens.astype(F32)
    token_scale = lax.rsqrt(jnp.mean(residual * residual, axis=-1, keepdims=True) + EPS)
    gained = (residual * attn_gain).astype(BF)
    message = gained.reshape(rows, NZ, block).transpose(1, 0, 2)
    message = jnp.concatenate((message, jnp.broadcast_to(meta[None], (NZ, 8, block))), axis=1)
    arrived = exchange(message, "z")
    spread = arrived[:, :rows].reshape(NZ * rows, block)
    route_rows = jnp.sum(arrived[:, rows:, : NZ * rows].astype(F32), axis=0)

    part = jnp.dot(spread, qkv_weight, preferred_element_type=F32).astype(BF)
    summed = exchange(part.reshape(NZ, rows, 3 * cols), "z").astype(F32).sum(axis=0) * token_scale

    def heads_of(values):
        return values.reshape(rows, heads, size)

    query_unit = unit_rows(heads_of(summed[:, :cols])) * size ** (-0.5)
    key_unit = unit_rows(heads_of(summed[:, cols : 2 * cols]))
    value_heads = heads_of(summed[:, 2 * cols :])
    decay_cols = lax.dynamic_slice_in_dim(decay_weight, ti * heads, heads, 1)
    beta_cols = lax.dynamic_slice_in_dim(beta_weight, ti * heads, heads, 1)
    decay_pre = jnp.dot(gained, decay_cols, preferred_element_type=F32) * token_scale
    beta_pre = jnp.dot(gained, beta_cols, preferred_element_type=F32) * token_scale
    decay = jnp.exp(-decay_rate * jax.nn.softplus(decay_pre))
    beta_gate = jax.nn.sigmoid(beta_pre)
    recalled = jnp.einsum("bhk,bhkv->bhv", key_unit, delta_state)
    correction = beta_gate[..., None] * (value_heads - decay[..., None] * recalled)
    new_state = (
        decay[..., None, None] * delta_state + key_unit[..., :, None] * correction[..., None, :]
    )
    read_out = jnp.einsum("bhk,bhkv->bhv", query_unit, new_state)
    head_out = rms_scale(read_out, head_gain).astype(BF).reshape(rows, cols)
    attn_part = jnp.dot(head_out, output_weight, preferred_element_type=F32).astype(BF)
    attn_part = attn_part.reshape(rows, NT, block).transpose(1, 0, 2)
    attn_sum = exchange(attn_part, ("y", "c")).astype(F32).sum(axis=0)
    own_tokens = lax.dynamic_slice_in_dim(tokens, ti * block, block, 1)
    middle = own_tokens.astype(F32) + attn_sum

    mid = gathered(middle.astype(BF), "z").reshape(NZ * rows, block)
    own_gain = lax.dynamic_slice_in_dim(ffn_gain, ti * block, block, 0)
    mid_wide = mid.astype(F32)
    square = jnp.sum(mid_wide * mid_wide, axis=1).reshape(NT, rows)
    square_high, square_low = two_parts(square)
    scaled = (mid_wide * own_gain).astype(BF)
    dense_part = jnp.einsum("nd,xdf->xnf", scaled, gate_up, preferred_element_type=F32).astype(BF)
    dense_part = dense_part.reshape(NX, NT, rows, 2 * half)

    code = route_rows[:2].astype(jnp.int32) - zi * (NX * CAP)
    token_z = jnp.arange(NZ * rows, dtype=jnp.int32) // rows
    slot = (code // CAP) * (NZ * CAP) + token_z[None] * CAP + code % CAP
    slot = jnp.where((code >= 0) & (code < NX * CAP), slot, -1)
    slots = NX * NZ * CAP
    hits = jnp.arange(slots, dtype=jnp.int32)[None, :, None] == slot[:, None, :]
    dispatch = (hits[0] | hits[1]).astype(BF)
    chosen = jnp.dot(dispatch, mid, preferred_element_type=F32).astype(BF)
    chosen = chosen.reshape(NX, 1, NZ * CAP, 2, block // 2)
    chosen = jnp.broadcast_to(chosen, (NX, NT, NZ * CAP, 2, block // 2))
    squares = jnp.stack((square_high, square_low), axis=1)
    squares = jnp.pad(squares, ((0, 0), (0, 6), (0, 2 * half - rows)))
    squares = jnp.broadcast_to(squares[None], (NX, NT, 8, 2 * half))
    message = jnp.concatenate(
        (chosen[:, :, :, 0], chosen[:, :, :, 1], dense_part, squares), axis=2
    )
    message = message.reshape(NX * NT, *message.shape[2:])
    arrived = exchange(message, ("x", "y", "c")).reshape(NX, NT, *message.shape[1:])
    per = NZ * CAP
    routed = arrived[:, :, : 2 * per].reshape(NX, NT, 2, per, block // 2)
    routed = routed.transpose(0, 3, 1, 2, 4).reshape(NX * per, width).astype(F32)
    routed_scale = lax.rsqrt(jnp.mean(routed * routed, axis=1, keepdims=True) + EPS)
    routed = (routed * routed_scale * ffn_gain).astype(BF)
    gate_vals = jnp.dot(routed, expert_gate[0], preferred_element_type=F32)
    up_vals = jnp.dot(routed, expert_up[0], preferred_element_type=F32)
    hidden = (jax.nn.silu(gate_vals) * up_vals).astype(BF)
    result = jnp.dot(hidden, expert_down[0], preferred_element_type=F32).astype(BF)
    result = result.reshape(NX, per, NT, block).transpose(0, 2, 1, 3)

    dense_sum = arrived[:, :, 2 * per : 2 * per + rows].astype(F32).sum(axis=1)
    square_sum = arrived[:, :, 2 * per + rows : 2 * per + rows + 2, :rows].astype(F32).sum(axis=(1, 2))
    dense_scale = lax.rsqrt(square_sum / width + EPS)
    dense_sum = dense_sum * dense_scale[:, :, None]
    dense_hidden = (jax.nn.silu(dense_sum[..., :half]) * dense_sum[..., half:]).astype(BF)
    dense_hidden = jnp.broadcast_to(dense_hidden[:, None], (NX, NT, rows, half))
    message = jnp.concatenate((result, dense_hidden), axis=3).reshape(NX * NT, rows, block + half)
    arrived = exchange(message, ("x", "y", "c")).reshape(NX, NT, rows, block + half)
    expert_sum = arrived[..., :block].astype(F32).sum(axis=1).astype(BF).reshape(slots, block)
    dense_in = arrived[..., block:].reshape(NX, NT * rows, half)
    dense_out = jnp.einsum("xnf,xfd->nd", dense_in, down, preferred_element_type=F32)
    mix_high = jnp.where(hits[0], route_rows[2], jnp.where(hits[1], route_rows[3], 0)).astype(BF)
    mix_low = jnp.where(hits[0], route_rows[4], jnp.where(hits[1], route_rows[5], 0)).astype(BF)
    over_slots = (((0,), (0,)), ((), ()))
    expert_mix = lax.dot_general(mix_high, expert_sum, over_slots, preferred_element_type=F32)
    expert_mix += lax.dot_general(mix_low, expert_sum, over_slots, preferred_element_type=F32)
    mixed = (jax.nn.sigmoid(dense_mix) * dense_out + expert_mix).astype(BF)
    mixed = exchange(mixed.reshape(NZ, rows, block), "z").astype(F32).sum(axis=0)
    return ((middle + mixed).astype(BF), new_state)


def solution(mesh):
    fine = Mesh(mesh.devices.reshape(NZ, NX, 4, 2), ("z", "x", "y", "c"))
    ep, tp = ("z", "x"), ("y", "c")
    return jax.shard_map(
        per_device,
        mesh=fine,
        in_specs=(
            P(ep, None),
            P(ep, tp, None, None),
            P(),
            P(ep, tp),
            P(ep, tp),
            P(ep, tp),
            P(),
            P(),
            P(tp),
            P(),
            P(tp, None),
            P(),
            P(ep, None),
            P(ep),
            P(ep, None),
            P(ep, None, tp),
            P(ep, None, tp),
            P(ep, tp, None),
            P(tp, ep),
            P(tp, ep),
            P(ep, tp),
            P(tp),
        ),
        out_specs=(P(ep, tp), P(ep, tp, None, None)),
        check_vma=False,
    )
```

time: 271 us -> 195 us (0.72)
  waiting for transfers between devices: 161 us -> 91.8 us
  blocking collectives: 21.2 us -> 14.4 us
  matrix products: 19.1 us -> 14.9 us
    all_to_all x8, waiting for transfers between devices: 161 us -> 91.8 us  [exchange(): return lax.all_to_all(tiles, axes, split_axis=0, concat_axis=0, tiled=True)]
    all_to_all x1, blocking collectives: 21.2 us -> 14.4 us  [exchange(): return lax.all_to_all(tiles, axes, split_axis=0, concat_axis=0, tiled=True)]
    dot_general x9 -> x12, matrix products: 16 us -> 11.8 us  [the longest x1 3.13 us: per_device(): jnp.dot(hidden, expert_down[0], preferred_element_type=F32).astype(BF)]
    convert_element_type x0 -> x2, local copies, waits for them, and re-layouts: none -> 3.94 us  [per_device(): routed = (routed * routed_scale * ffn_gain).astype(BF)]
    reshape x8 -> x5, local copies, waits for them, and re-layouts: 4.59 us -> 0.98 us  [the longest x1 0.68 us: per_device(): attn_part = attn_part.reshape(rows, NT, block).transpose(1, 0, 2)]
    broadcast_in_dim x4 -> x14, local copies, waits for them, and re-layouts: 6.21 us -> 3.26 us  [the longest x3 2.86 us: gathered(): return exchange(jnp.broadcast_to(shard[None], (count, *shard.shape)), axis)]
  transfers between devices with their start and end apart: 8 -> 8, of which waited for: 8 -> 8; matrix products, arithmetic and copies ran while one was open for 8% -> 3% of each run, Pallas kernels for 0% -> 0%
where the time goes in v1:
time: 195 us; the launch traced here: 192 us
  waiting for transfers between devices  91.8 us (47%)
  starting transfers between devices  42 us (22%)
  matrix products  14.9 us (8%)
  local copies, waits for them, and re-layouts  14.6 us (7%)
  blocking collectives  14.4 us (7%)
  other arithmetic  12.6 us (6%)
    all_to_all x8, waiting for transfers between devices, exchange(): return lax.all_to_all(tiles, axes, split_axis=0, concat_axis=0, tiled=True)  91.8 us
    all_to_all x8, starting transfers between devices, exchange(): return lax.all_to_all(tiles, axes, split_axis=0, concat_axis=0, tiled=True)  42 us
    all_to_all x1, blocking collectives, exchange(): return lax.all_to_all(tiles, axes, split_axis=0, concat_axis=0, tiled=True)  14.4 us
    convert_element_type x2, local copies, waits for them, and re-layouts, per_device(): routed = (routed * routed_scale * ffn_gain).astype(BF)  3.94 us
  transfers between devices with their start and end apart: 8, of which 8 were waited for; matrix products, arithmetic and copies ran while one was open for 3% of the time, Pallas kernels for 0%

profile of v1, /device:TPU:2, one launch (start us, length us, event | category | flops | bytes accessed | tf_op | source)
XLA Modules:
  0.0 191.6 jit_solution(5135174570323535800)
XLA Ops:
  0.9 0.8 exponential_reduce_fusion
  1.7 0.8 copy.128
  2.5 0.1 fusion.7
  2.7 0.1 reduce_sum.143
  3.0 0.7 fusion.68
  3.7 0.7 fusion.66
  4.5 1.6 fusion.23
  6.3 0.8 copy.130
  7.1 8.5 %all-to-all-start = ((bf16[8,32,512]{2,1,0:T(8,128)(2,1)}), bf16[8,32,512]{2,1,0:T(8,128)(2,1)S(1)}, u32[]{:S(2)}, u32[]{:S(2)}) async-start(bf16[8,32,512]{2,1,0:T(8,128)(2,1)} %copy.130), calls=%async_computation | async-start | bytes 524288 | tf_op jit(solution)/shard_map/all_to_all | solution.py:14
  15.6 11.8 %all-to-all-done = bf16[8,32,512]{2,1,0:T(8,128)(2,1)S(1)} async-done(((bf16[8,32,512]{2,1,0:T(8,128)(2,1)}), bf16[8,32,512]{2,1,0:T(8,128)(2,1)S(1)}, u32[]{:S(2)}, u32[]{:S(2)}) %all-to-all-start) | async-done | bytes 262176 | tf_op jit(solution)/shard_map/all_to_all | solution.py:14
  27.4 0.9 broadcast_in_dim.142
  28.3 5.0 %all-to-all-start.1 = ((bf16[4,128,768]{2,1,0:T(8,128)(2,1)}), bf16[4,128,768]{2,1,0:T(8,128)(2,1)S(1)}, u32[]{:S(2)}, u32[]{:S(2)}) async-start(bf16[4,128,768]{2,1,0:T(8,128)(2,1)} %broadcast_in_dim.142), calls=%async_computation.1 | async-start | bytes 1572864 | tf_op jit(solution)/shard_map/all_to_all | solution.py:14
  33.3 9.2 %all-to-all-done.1 = bf16[4,128,768]{2,1,0:T(8,128)(2,1)S(1)} async-done(((bf16[4,128,768]{2,1,0:T(8,128)(2,1)}), bf16[4,128,768]{2,1,0:T(8,128)(2,1)S(1)}, u32[]{:S(2)}, u32[]{:S(2)}) %all-to-all-start.1) | async-done | bytes 786464 | tf_op jit(solution)/shard_map/all_to_all | solution.py:14
  42.5 1.0 convolution_convert_fusion.3
  43.5 3.4 %all-to-all-start.2 = ((bf16[8,24,768]{2,1,0:T(8,128)(2,1)}), bf16[8,24,768]{2,1,0:T(8,128)(2,1)S(1)}, u32[]{:S(2)}, u32[]{:S(2)}) async-start(bf16[8,24,768]{2,1,0:T(8,128)(2,1)} %bitcast.6), calls=%async_computation.2 | async-start | bytes 589824 | tf_op jit(solution)/shard_map/all_to_all | solution.py:14
  46.9 0.7 add_rsqrt_fusion.5
  47.6 0.7 neg.21
  48.3 1.0 fusion.61
  49.4 1.0 fusion.11
  50.5 0.1 dynamic_slice.15
  50.6 7.1 %all-to-all-done.2 = bf16[8,24,768]{2,1,0:T(8,128)(2,1)S(1)} async-done(((bf16[8,24,768]{2,1,0:T(8,128)(2,1)}), bf16[8,24,768]{2,1,0:T(8,128)(2,1)S(1)}, u32[]{:S(2)}, u32[]{:S(2)}) %all-to-all-start.2) | async-done | bytes 294944 | tf_op jit(solution)/shard_map/all_to_all | solution.py:14
  58.3 2.6 %fusion.78 = f32[24,2,1,128]{3,2,1,0:T(1,128)S(1)} fusion(f32[24,2,128,1]{2,3,1,0:T(1,128)S(1)} %bitcast.136, f32[24,2,128,128]{3,2,1,0:T(8,128)} %param.23), kind=kOutput, calls=%fused_computation.150 | convolution fusion | flops 1572864 | bytes 3194880 | tf_op jit(solution)/shard_map/bhk,bhkv->bhv/dot_general | solution.py:123
  60.9 0.1 subtract_multiply_fusion
  61.0 0.1 copy-done.1
  61.2 1.1 multiply_add_fusion
  62.3 0.5 fusion.79
  62.8 0.1 multiply_reduce_fusion.1
  63.1 0.4 convolution_convert_fusion.1
  63.4 0.5 copy-done.2
  63.9 0.7 copy.163
  64.6 4.5 %all-to-all-start.3 = ((bf16[8,24,512]{2,1,0:T(8,128)(2,1)}), bf16[8,24,512]{2,1,0:T(8,128)(2,1)S(1)}, u32[]{:S(2)}, u32[]{:S(2)}) async-start(bf16[8,24,512]{2,1,0:T(8,128)(2,1)} %bitcast.108), calls=%async_computation.3 | async-start | bytes 393216 | tf_op jit(solution)/shard_map/all_to_all | solution.py:14
  69.1 6.8 %all-to-all-done.3 = bf16[8,24,512]{2,1,0:T(8,128)(2,1)S(1)} async-done(((bf16[8,24,512]{2,1,0:T(8,128)(2,1)}), bf16[8,24,512]{2,1,0:T(8,128)(2,1)S(1)}, u32[]{:S(2)}, u32[]{:S(2)}) %all-to-all-start.3) | async-done | bytes 196640 | tf_op jit(solution)/shard_map/all_to_all | solution.py:14
  75.9 0.8 fusion.48
  76.7 0.7 broadcast_in_dim.143
  77.3 3.4 %all-to-all-start.4 = ((bf16[8,24,512]{2,1,0:T(8,128)(2,1)}), bf16[8,24,512]{2,1,0:T(8,128)(2,1)S(1)}, u32[]{:S(2)}, u32[]{:S(2)}) async-start(bf16[8,24,512]{2,1,0:T(8,128)(2,1)} %broadcast_in_dim.143), calls=%async_computation.4 | async-start | bytes 393216 | tf_op jit(solution)/shard_map/all_to_all | solution.py:14
  80.8 10.3 %all-to-all-done.4 = bf16[8,24,512]{2,1,0:T(8,128)(2,1)S(1)} async-done(((bf16[8,24,512]{2,1,0:T(8,128)(2,1)}), bf16[8,24,512]{2,1,0:T(8,128)(2,1)S(1)}, u32[]{:S(2)}, u32[]{:S(2)}) %all-to-all-start.4) | async-done | bytes 196640 | tf_op jit(solution)/shard_map/all_to_all | solution.py:14
  91.1 1.2 broadcast_in_dim.149
  92.4 5.8 %all-to-all-start.5 = ((bf16[4,768,256]{2,1,0:T(8,128)(2,1)}), bf16[4,768,256]{2,1,0:T(8,128)(2,1)}, u32[]{:S(2)}, u32[]{:S(2)}) async-start(bf16[4,768,256]{2,1,0:T(8,128)(2,1)} %broadcast_in_dim.149), calls=%async_computation.5 | async-start | bytes 3145728 | tf_op jit(solution)/shard_map/all_to_all | solution.py:14
  98.2 0.1 multiply_reduce_fusion
  98.4 0.2 convolution_convert_fusion.4
  98.6 0.1 fusion.75
  98.8 17.3 %all-to-all-done.5 = bf16[4,768,256]{2,1,0:T(8,128)(2,1)} async-done(((bf16[4,768,256]{2,1,0:T(8,128)(2,1)}), bf16[4,768,256]{2,1,0:T(8,128)(2,1)}, u32[]{:S(2)}, u32[]{:S(2)}) %all-to-all-start.5) | async-done | bytes 1572896 | tf_op jit(solution)/shard_map/all_to_all | solution.py:14
  116.0 1.6 convolution_convert_fusion.2
  117.7 1.2 pad_maximum_fusion
  118.9 5.1 %all-to-all-start.6 = ((bf16[32,80,256]{2,1,0:T(8,128)(2,1)}), bf16[32,80,256]{2,1,0:T(8,128)(2,1)S(1)}, u32[]{:S(2)}, u32[]{:S(2)}) async-start(bf16[32,80,256]{2,1,0:T(8,128)(2,1)} %pad_maximum_fusion), calls=%async_computation.6 | async-start | bytes 2621440 | tf_op jit(solution)/shard_map/all_to_all | solution.py:14
  124.0 17.3 %all-to-all-done.6 = bf16[32,80,256]{2,1,0:T(8,128)(2,1)S(1)} async-done(((bf16[32,80,256]{2,1,0:T(8,128)(2,1)}), bf16[32,80,256]{2,1,0:T(8,128)(2,1)S(1)}, u32[]{:S(2)}, u32[]{:S(2)}) %all-to-all-start.6) | async-done | bytes 1310752 | tf_op jit(solution)/shard_map/all_to_all | solution.py:14
  141.5 0.2 fusion
  141.8 0.3 fusion.18
  142.1 1.5 copy.140
  143.6 2.4 %convert_element_type.181 = bf16[96,4096]{1,0:T(8,128)(2,1)S(1)} reshape(bf16[4,24,8,2,256]{4,3,2,1,0:T(2,128)(2,1)} %copy.140) | data formatting | bytes 1572864 | tf_op jit(solution)/shard_map/convert_element_type | solution.py:167
  146.0 1.6 fusion.16
  147.6 3.1 %convolution_convert_fusion = bf16[96,4096]{1,0:T(8,128)(2,1)} fusion(bf16[96,4096]{1,0:T(8,128)(2,1)S(1)} %convert_element_type.181, bf16[1,128,4096]{2,1,0:T(8,128)(2,1)} %param.39, bf16[1,4096,128]{2,1,0:T(8,128)(2,1)} %param.38, f32[96,128]{1,0:T(8,128)S(1)} %fusion.16), kind=kOutput, calls=%fused_computation | convolution fusion | flops 201793536 | bytes 3719168 | tf_op jit(solution)/shard_map/dot_general | solution.py:171
  150.8 1.4 copy.153
  152.2 0.2 copy.162
  152.5 1.0 pad_maximum_fusion.1
  153.5 6.4 %all-to-all-start.7 = ((bf16[32,24,640]{2,1,0:T(8,128)(2,1)}), bf16[32,24,640]{2,1,0:T(8,128)(2,1)S(1)}, u32[]{:S(2)}, u32[]{:S(2)}) async-start(bf16[32,24,640]{2,1,0:T(8,128)(2,1)} %bitcast.118), calls=%async_computation.7 | async-start | bytes 1966080 | tf_op jit(solution)/shard_map/all_to_all | solution.py:14
  159.9 1.8 fusion.73
  161.7 12.1 %all-to-all-done.7 = bf16[32,24,640]{2,1,0:T(8,128)(2,1)S(1)} async-done(((bf16[32,24,640]{2,1,0:T(8,128)(2,1)}), bf16[32,24,640]{2,1,0:T(8,128)(2,1)S(1)}, u32[]{:S(2)}, u32[]{:S(2)}) %all-to-all-start.7) | async-done | bytes 983072 | tf_op jit(solution)/shard_map/all_to_all | solution.py:14
  173.8 0.1 slice_reduce_fusion
  174.0 0.2 fusion.32
  174.2 1.2 fusion.3
  175.5 0.3 fusion.5
  175.7 14.4 %all_to_all.45 = bf16[8,24,512]{2,1,0:T(8,128)(2,1)S(1)} all-to-all(bf16[8,24,512]{2,1,0:T(8,128)(2,1)S(1)} %bitcast.133), channel_id=1, replica_groups=mesh['z'=8,'x'=4,'y'=4,'c'=2] {'z'}, dimensions={0} | all-to-all | bytes 393216 | tf_op jit(solution)/shard_map/all_to_all | solution.py:14
  190.2 1.4 add_convert_fusion
  (85 shorter events, 2.3 us)
Async XLA Ops:
  0.6 62.4 %copy-start = (bf16[256,4096]{1,0:T(8,128)(2,1)S(1)}, bf16[256,4096]{1,0:T(8,128)(2,1)}, u32[]{:S(2)}) copy-start(bf16[256,4096]{1,0:T(8,128)(2,1)} %param.32) | copy-start | bytes 6291460
  0.6 14.9 %copy-start.6 = (bf16[128,256]{1,0:T(8,128)(2,1)S(1)}, bf16[128,256]{1,0:T(8,128)(2,1)}, u32[]{:S(2)}) copy-start(bf16[128,256]{1,0:T(8,128)(2,1)} %param.27) | copy-start | bytes 196612
  0.7 14.9 %copy-start.7 = (bf16[128,256]{1,0:T(8,128)(2,1)S(1)}, bf16[128,256]{1,0:T(8,128)(2,1)}, u32[]{:S(2)}) copy-start(bf16[128,256]{1,0:T(8,128)(2,1)} %param.26) | copy-start | bytes 196612
  0.7 14.9 %copy-start.8 = (bf16[128,256]{1,0:T(8,128)(2,1)S(1)}, bf16[128,256]{1,0:T(8,128)(2,1)}, u32[]{:S(2)}) copy-start(bf16[128,256]{1,0:T(8,128)(2,1)} %param.25) | copy-start | bytes 196612
  7.1 20.3 %all-to-all-start = ((bf16[8,32,512]{2,1,0:T(8,128)(2,1)}), bf16[8,32,512]{2,1,0:T(8,128)(2,1)S(1)}, u32[]{:S(2)}, u32[]{:S(2)}) async-start(bf16[8,32,512]{2,1,0:T(8,128)(2,1)} %copy.130), calls=%async_computation | async-start | bytes 524288 | tf_op jit(solution)/shard_map/all_to_all | solution.py:14
  28.3 22.2 %copy-start.9 = (f32[4096]{0:T(1024)S(1)}, f32[4096]{0:T(1024)}, u32[]{:S(2)}) copy-start(f32[4096]{0:T(1024)} %param.33) | copy-start | bytes 49156
  28.3 14.1 %all-to-all-start.1 = ((bf16[4,128,768]{2,1,0:T(8,128)(2,1)}), bf16[4,128,768]{2,1,0:T(8,128)(2,1)S(1)}, u32[]{:S(2)}, u32[]{:S(2)}) async-start(bf16[4,128,768]{2,1,0:T(8,128)(2,1)} %broadcast_in_dim.142), calls=%async_computation.1 | async-start | bytes 1572864 | tf_op jit(solution)/shard_map/all_to_all | solution.py:14
  43.5 14.2 %all-to-all-start.2 = ((bf16[8,24,768]{2,1,0:T(8,128)(2,1)}), bf16[8,24,768]{2,1,0:T(8,128)(2,1)S(1)}, u32[]{:S(2)}, u32[]{:S(2)}) async-start(bf16[8,24,768]{2,1,0:T(8,128)(2,1)} %bitcast.6), calls=%async_computation.2 | async-start | bytes 589824 | tf_op jit(solution)/shard_map/all_to_all | solution.py:14
  58.3 2.8 %copy-start.1 = (f32[24,2,128,128]{3,2,1,0:T(8,128)S(1)}, f32[24,2,128,128]{3,2,1,0:T(8,128)}, u32[]{:S(2)}) copy-start(f32[24,2,128,128]{3,2,1,0:T(8,128)} %param.23) | copy-start | bytes 9437188
  62.2 1.7 copy-start.2
  62.3 0.7 copy-start.11
  62.8 6.3 %copy-start.3 = (bf16[128,512]{1,0:T(8,128)(2,1)S(1)}, bf16[128,512]{1,0:T(8,128)(2,1)}, u32[]{:S(2)}) copy-start(bf16[128,512]{1,0:T(8,128)(2,1)} %param.42) | copy-start | bytes 393220
  63.0 17.7 %copy-start.4 = (bf16[512,128]{1,0:T(8,128)(2,1)S(1)}, bf16[512,128]{1,0:T(8,128)(2,1)}, u32[]{:S(2)}) copy-start(bf16[512,128]{1,0:T(8,128)(2,1)} %param.41) | copy-start | bytes 393220
  63.1 17.7 %copy-start.5 = (bf16[512,128]{1,0:T(8,128)(2,1)S(1)}, bf16[512,128]{1,0:T(8,128)(2,1)}, u32[]{:S(2)}) copy-start(bf16[512,128]{1,0:T(8,128)(2,1)} %param.40) | copy-start | bytes 393220
  64.6 11.3 %all-to-all-start.3 = ((bf16[8,24,512]{2,1,0:T(8,128)(2,1)}), bf16[8,24,512]{2,1,0:T(8,128)(2,1)S(1)}, u32[]{:S(2)}, u32[]{:S(2)}) async-start(bf16[8,24,512]{2,1,0:T(8,128)(2,1)} %bitcast.108), calls=%async_computation.3 | async-start | bytes 393216 | tf_op jit(solution)/shard_map/all_to_all | solution.py:14
  77.3 13.8 %all-to-all-start.4 = ((bf16[8,24,512]{2,1,0:T(8,128)(2,1)}), bf16[8,24,512]{2,1,0:T(8,128)(2,1)S(1)}, u32[]{:S(2)}, u32[]{:S(2)}) async-start(bf16[8,24,512]{2,1,0:T(8,128)(2,1)} %broadcast_in_dim.143), calls=%async_computation.4 | async-start | bytes 393216 | tf_op jit(solution)/shard_map/all_to_all | solution.py:14
  92.4 23.6 %all-to-all-start.5 = ((bf16[4,768,256]{2,1,0:T(8,128)(2,1)}), bf16[4,768,256]{2,1,0:T(8,128)(2,1)}, u32[]{:S(2)}, u32[]{:S(2)}) async-start(bf16[4,768,256]{2,1,0:T(8,128)(2,1)} %broadcast_in_dim.149), calls=%async_computation.5 | async-start | bytes 3145728 | tf_op jit(solution)/shard_map/all_to_all | solution.py:14
  118.9 22.4 %all-to-all-start.6 = ((bf16[32,80,256]{2,1,0:T(8,128)(2,1)}), bf16[32,80,256]{2,1,0:T(8,128)(2,1)S(1)}, u32[]{:S(2)}, u32[]{:S(2)}) async-start(bf16[32,80,256]{2,1,0:T(8,128)(2,1)} %pad_maximum_fusion), calls=%async_computation.6 | async-start | bytes 2621440 | tf_op jit(solution)/shard_map/all_to_all | solution.py:14
  152.4 7.5 %copy-start.10 = (f32[512]{0:T(512)S(1)}, f32[512]{0:T(512)}, u32[]{:S(2)}) copy-start(f32[512]{0:T(512)} %param.43) | copy-start | bytes 6148
  153.5 20.3 %all-to-all-start.7 = ((bf16[32,24,640]{2,1,0:T(8,128)(2,1)}), bf16[32,24,640]{2,1,0:T(8,128)(2,1)S(1)}, u32[]{:S(2)}, u32[]{:S(2)}) async-start(bf16[32,24,640]{2,1,0:T(8,128)(2,1)} %bitcast.118), calls=%async_computation.7 | async-start | bytes 1966080 | tf_op jit(solution)/shard_map/all_to_all | solution.py:14
